TPU v7x, 128 devices: a 2x2x16 block of a 8x8x16 slice. The times are simulated.
128 devices in a mesh: grp: 4 (over y, x), ep: 32 (over z, core).
Axes of the slice: x: 2, y: 2, z: 16, core: 2. Of those that a mesh axis runs over, the one named last changes fastest.
The devices are a block of a 8x8x16 slice.
Arguments:
- residual_input: bfloat16 [3072, 2048], P(('grp', 'ep')), parts along dimension 0, may hold values from -6 to 6
- attention_norm_gain: bfloat16 [2048], replicated, may hold values from 0.099609375 to 1.8984375
- receptance_weight: bfloat16 [2048, 1024], P(None, 'ep'), may hold values from -0.125 to 0.125
- key_weight: bfloat16 [2048, 1024], P(None, 'ep'), may hold values from -0.125 to 0.125
- value_weight: bfloat16 [2048, 1024], P(None, 'ep'), may hold values from -0.125 to 0.125
- decay_weight: bfloat16 [2048, 1024], P(None, 'ep'), may hold values from -0.125 to 0.125
- correction_rate_weight: bfloat16 [2048, 1024], P(None, 'ep'), may hold values from -0.125 to 0.125
- output_gate_weight: bfloat16 [2048, 1024], P(None, 'ep'), may hold values from -0.125 to 0.125
- decay_offset: float32 [1024], replicated, may hold values from -3 to 1
- correction_rate_offset: float32 [1024], replicated, may hold values from -1.5 to 1.5
- self_term_weight: float32 [1024], replicated, may hold values from -2 to 2
- head_read_gain: float32 [1024], replicated, may hold values from 0.1 to 1.9
- previous_state: float32 [3072, 16, 4096], P(('grp', 'ep')), parts along dimension 0, may hold values from -4 to 4
- attention_output_weight: bfloat16 [1024, 2048], replicated, may hold values from -0.1875 to 0.1875
- feedforward_norm_gain: bfloat16 [2048], replicated, may hold values from 0.099609375 to 1.8984375
- routes: int32 [3072, 4], P('grp'), parts along dimension 0, may hold values from 0 to 31, all different within a row; in each aligned block of 24 rows (0 to 23, 24 to 47, ...) at most 4 rows name the same one
- routing_weight: float32 [3072, 4], P('grp'), parts along dimension 0, may hold values from 0.2 to 1
- routed_gate_weight: bfloat16 [32, 2048, 512], P('ep'), may hold values from -0.125 to 0.125
- routed_up_weight: bfloat16 [32, 2048, 512], P('ep'), may hold values from -0.125 to 0.125
- routed_down_weight: bfloat16 [32, 512, 2048], P('ep'), may hold values from -0.25 to 0.25
- common_gate_weight: bfloat16 [2048, 512], replicated, may hold values from -0.125 to 0.125
- common_up_weight: bfloat16 [2048, 512], replicated, may hold values from -0.125 to 0.125
- common_down_weight: bfloat16 [512, 2048], replicated, may hold values from -0.25 to 0.25
Outputs:
- hidden_out: bfloat16 [3072, 2048], P(('grp', 'ep')), parts along dimension 0
- next_state: float32 [3072, 16, 4096], P(('grp', 'ep')), parts along dimension 0
There are 4 independent parts, one for each index of `grp`. A program takes and returns all parts, laid end to end along the dimension named above; an argument that names none is the same for every part. Nothing has to cross between parts.
Inputs may be any that keep to these rules, and one draw needn't show every extreme that they name: `routes`: the 4 entries of a row differ. In each aligned block of 24 rows (the tokens of one index of ep) no expert is named by more than 4 rows, a bound that some block reaches.
All inputs are finite; a program needn't handle non-finite values.
Results may differ from a plain program's by a relative error of at most 0.013.
Values may be sent and summed in bfloat16 or wider, within the bound.
A program may use at most 128 MiB of HBM per device.

v0:
```python
import jax
import jax.numpy as jnp
from jax import lax
from jax.sharding import PartitionSpec as P

HEAD_COUNT = 16
HEAD_SIZE = 64
CAP = 4


def rms_norm(value_rows, gain):
    scale = lax.rsqrt(jnp.mean(value_rows * value_rows, axis=-1, keepdims=True) + 1e-06)
    return (value_rows * scale * gain.astype(jnp.float32)).astype(jnp.bfloat16)


def expert_mlp(rows, gate_w, up_w, down_w):
    gate = jnp.dot(rows, gate_w, preferred_element_type=jnp.float32)
    upward = jnp.dot(rows, up_w, preferred_element_type=jnp.float32)
    hidden = (jax.nn.silu(gate) * upward).astype(jnp.bfloat16)
    return jnp.dot(hidden, down_w, preferred_element_type=jnp.float32).astype(jnp.bfloat16)


def attention_mixer(
    receptance_rows,
    key_rows,
    value_rows,
    decay_logit,
    rate_logit,
    gate_logit,
    decay_offset,
    correction_rate_offset,
    self_term_weight,
    head_read_gain,
    head_state,
):
    tally_value = receptance_rows.shape[0]

    def heads(tensor):
        return tensor.astype(jnp.float32).reshape(tally_value, HEAD_COUNT, HEAD_SIZE)

    decay = jnp.exp(
        -jnp.exp(-jax.nn.softplus(-(decay_offset + decay_logit.astype(jnp.float32))) - 0.5)
    )
    rate = jax.nn.sigmoid(correction_rate_offset + rate_logit.astype(jnp.float32))
    key_head = heads(key_rows)
    rate_head = heads(rate)
    receptance_head = heads(receptance_rows)
    head_value = heads(value_rows)
    unit_key = key_head * lax.rsqrt(1.0 + jnp.sum(key_head * key_head, axis=-1, keepdims=True))
    rate_scaled_key = key_head * rate_head
    removal = unit_key * rate_head
    matrix = head_state.reshape(tally_value, HEAD_COUNT, HEAD_SIZE, HEAD_SIZE)
    recalled = jnp.einsum("nhvk,nhk->nhv", matrix, unit_key)
    matrix = (
        matrix * heads(decay)[:, :, None, :]
        - recalled[..., None] * removal[:, :, None, :]
        + head_value[..., None] * rate_scaled_key[:, :, None, :]
    )
    read = jnp.einsum("nhvk,nhk->nhv", matrix, receptance_head)
    centered = read - jnp.mean(read, axis=-1, keepdims=True)
    variance = jnp.mean(centered * centered, axis=-1, keepdims=True)
    normed_head_read = (
        centered * lax.rsqrt(variance + 0.00064) * head_read_gain.reshape(HEAD_COUNT, HEAD_SIZE)
    )
    self_term = (
        jnp.sum(
            receptance_head * rate_scaled_key * self_term_weight.reshape(HEAD_COUNT, HEAD_SIZE),
            axis=-1,
            keepdims=True,
        )
        * head_value
    )
    normed_mixer_input = (normed_head_read + self_term).reshape(
        tally_value, HEAD_COUNT * HEAD_SIZE
    ) * jax.nn.sigmoid(gate_logit.astype(jnp.float32))
    return (
        normed_mixer_input.astype(jnp.bfloat16),
        matrix.reshape(tally_value, HEAD_COUNT, HEAD_SIZE * HEAD_SIZE),
    )


def slot_table(block_routes, block_weight, expert_ids):
    match = block_routes[..., None] == expert_ids
    hit = jnp.any(match, axis=-2).astype(jnp.int32)
    weight = jnp.sum(jnp.where(match, block_weight[..., None], 0.0), axis=-2)
    rank = jnp.cumsum(hit, axis=-2) - hit
    slots = jnp.arange(CAP, dtype=jnp.int32)
    select = ((hit[..., None] == 1) & (rank[..., None] == slots)).astype(jnp.float32)
    return (select, weight)


def combine_returned(select, weight, returned):
    coefficient = select * weight[..., None]
    return jnp.einsum("nec,ecd->nd", coefficient, returned.astype(jnp.float32))


def per_device(
    residual_input,
    attention_norm_gain,
    receptance_weight,
    key_weight,
    value_weight,
    decay_weight,
    correction_rate_weight,
    output_gate_weight,
    decay_offset,
    correction_rate_offset,
    self_term_weight,
    head_read_gain,
    previous_state,
    attention_output_weight,
    feedforward_norm_gain,
    routes,
    routing_weight,
    routed_gate_weight,
    routed_up_weight,
    routed_down_weight,
    common_gate_weight,
    common_up_weight,
    common_down_weight,
):
    ep_size = lax.axis_size("ep")
    device = lax.axis_index("ep")
    tally_value = residual_input.shape[0]
    normed = rms_norm(residual_input.astype(jnp.float32), attention_norm_gain)
    stacked = jnp.stack(
        (
            receptance_weight,
            key_weight,
            value_weight,
            decay_weight,
            correction_rate_weight,
            output_gate_weight,
        ),
        axis=1,
    )
    local_cols = jnp.einsum(
        "td,drc->trc",
        lax.all_gather(normed, "ep", axis=0, tiled=True),
        stacked,
        preferred_element_type=jnp.float32,
    ).astype(jnp.bfloat16)
    role_rows = lax.all_to_all(local_cols, "ep", split_axis=0, concat_axis=2, tiled=True)
    normed_mixer_input, next_state = attention_mixer(
        role_rows[:, 0],
        role_rows[:, 1],
        role_rows[:, 2],
        role_rows[:, 3],
        role_rows[:, 4],
        role_rows[:, 5],
        decay_offset,
        correction_rate_offset,
        self_term_weight,
        head_read_gain,
        previous_state,
    )
    attended = jnp.dot(
        normed_mixer_input, attention_output_weight, preferred_element_type=jnp.float32
    ).astype(jnp.bfloat16)
    middle = residual_input.astype(jnp.float32) + attended.astype(jnp.float32)
    normed_ffn = rms_norm(middle, feedforward_norm_gain)
    shared = expert_mlp(normed_ffn, common_gate_weight, common_up_weight, common_down_weight)
    expert_count = routed_gate_weight.shape[0] * ep_size
    all_ids = jnp.arange(expert_count, dtype=jnp.int32)
    own_routes = lax.dynamic_slice_in_dim(routes, device * tally_value, tally_value, 0)
    own_weight = lax.dynamic_slice_in_dim(routing_weight, device * tally_value, tally_value, 0)
    select, weight = slot_table(own_routes, own_weight, all_ids)
    dispatch = jnp.einsum(
        "nec,nd->ecd", select.astype(jnp.bfloat16), normed_ffn, preferred_element_type=jnp.float32
    ).astype(jnp.bfloat16)
    received = lax.all_to_all(dispatch, "ep", split_axis=0, concat_axis=0, tiled=True)
    rows = received.reshape(-1, received.shape[-1])
    output = expert_mlp(
        rows, routed_gate_weight[0], routed_up_weight[0], routed_down_weight[0]
    ).reshape(received.shape)
    returned = lax.all_to_all(output, "ep", split_axis=0, concat_axis=0, tiled=True)
    routed = combine_returned(select, weight, returned)
    hidden_out = (middle + shared.astype(jnp.float32) + routed).astype(jnp.bfloat16)
    return (hidden_out, next_state)


def solution(mesh):
    return jax.shard_map(
        per_device,
        mesh=mesh,
        in_specs=(
            P(("grp", "ep"), None),
            P(),
            P(None, "ep"),
            P(None, "ep"),
            P(None, "ep"),
            P(None, "ep"),
            P(None, "ep"),
            P(None, "ep"),
            P(),
            P(),
            P(),
            P(),
            P(("grp", "ep"), None, None),
            P(),
            P(),
            P("grp", None),
            P("grp", None),
            P("ep", None, None),
            P("ep", None, None),
            P("ep", None, None),
            P(),
            P(),
            P(),
        ),
        out_specs=(P(("grp", "ep"), None), P(("grp", "ep"), None, None)),
        check_vma=False,
    )
```

profile of v0, /device:TPU:86, one launch (start us, length us, event | category | flops | bytes accessed | tf_op | source)
XLA Modules:
  0.0 277.2 jit_solution(2123901114076902468)
XLA Ops:
  8.1 1.0 fusion.34
  9.1 1.6 fusion.36
  16.3 69.5 %all-gather.2.cloned.1.call-done = bf16[768,2048]{1,0:T(8,128)(2,1)} async-done(((bf16[24,2048]{1,0:T(8,128)(2,1)}), bf16[768,2048]{1,0:T(8,128)(2,1)}) %all-gather.2.cloned.1.call-update) | async-done | bytes 3145744 | tf_op jit(solution)/shard_map/all_gather | solution.py:139
  85.8 3.1 %fusion.73 = f32[768,192]{0,1:S(1)} fusion(bf16[768,2048]{1,0:T(8,128)(2,1)} %all-gather.2.cloned.1.call-done, bf16[2048,192]{0,1:T(8,128)(2,1)S(1)} %bitcast.97), kind=kOutput, calls=%fused_computation.108 | convolution fusion | flops 603979776 | bytes 4521984
  89.0 1.8 copy.40
  90.8 3.4 %reshape.206 = bf16[32,2,2304]{2,1,0:T(2,128)(2,1)} reshape(bf16[768,6,32]{2,1,0:T(8,128)(2,1)} %copy.40) | data formatting | bytes 589824
  94.2 9.4 %all-to-all-start = ((bf16[32,2,2304]{2,1,0:T(2,128)(2,1)}), bf16[32,2,2304]{2,1,0:T(2,128)(2,1)S(1)}, u32[]{:S(2)}, u32[]{:S(2)}) async-start(bf16[32,2,2304]{2,1,0:T(2,128)(2,1)} %reshape.206), calls=%async_computation | async-start | bytes 589824 | tf_op jit(solution)/shard_map/all_to_all | solution.py:143
  103.7 10.9 %reshape.185 = f32[24,16,64,64]{3,2,1,0:T(8,128)} reshape(f32[24,16,4096]{2,1,0:T(8,128)} %param.35) | data formatting | bytes 12582912 | tf_op jit(solution)/shard_map/reshape | solution.py:52
  117.6 9.3 %all-to-all-done = bf16[32,2,2304]{2,1,0:T(2,128)(2,1)S(1)} async-done(((bf16[32,2,2304]{2,1,0:T(2,128)(2,1)}), bf16[32,2,2304]{2,1,0:T(2,128)(2,1)S(1)}, u32[]{:S(2)}, u32[]{:S(2)}) %all-to-all-start) | async-done | bytes 294944 | tf_op jit(solution)/shard_map/all_to_all | solution.py:143
  126.8 2.2 reshape.207
  129.0 2.2 copy.42
  131.2 1.9 all_to_all.22
  133.1 0.9 slice_convert_fusion.2
  137.2 8.1 %fusion.74 = f32[24,16,1,64]{3,2,1,0:T(1,128)S(1)} fusion(f32[24,16,64,1]{2,3,1,0:T(1,128)S(1)} %bitcast.95, f32[24,16,64,64]{3,2,1,0:T(8,128)} %reshape.185), kind=kOutput, calls=%fused_computation.109 | convolution fusion | flops 3145728 | bytes 6488064 | tf_op jit(solution)/shard_map/nhvk,nhk->nhv/dot_general | solution.py:53
  145.4 9.6 %fusion.1 = f32[24,16,1,64]{3,2,1,0:T(1,128)S(1)} fusion(bf16[24,16,64,1]{2,3,1,0:T(2,128)(2,1)S(1)} %copy-done.7, f32[24,16,64,64]{3,2,1,0:T(8,128)S(1)} %copy-done.1, f32[24,16,64]{2,1,0:T(8,128)S(1)} %fusion.41, f32[24,16,64]{2,1,0:T(8,128)S(1)} %get-tuple-element.2, f32[24,16,64]{2,1,0:T(8,128)S(1)} %bitcast.93, f32[24,16,64]{2,1,0:T(8,128)S(1)} %get-tuple-element.4, ...), kind=kOutput, calls=%fused_computation.1 | convolution fusion | flops 11010048 | bytes 6930432 | tf_op jit(solution)/shard_map/nhvk,nhk->nhv/dot_general | solution.py:59
  156.3 3.0 %multiply_reduce_fusion = (f32[24]{0:T(128)S(1)}, f32[24,2048]{1,0:T(8,128)S(1)}) fusion(bf16[1024,2048]{1,0:T(8,128)(2,1)} %param.36, f32[24,1024]{1,0:T(8,128)S(1)} %reshape.187, bf16[24,6,1024]{2,0,1:T(8,128)(2,1)} %all_to_all.22, bf16[24,2048]{1,0:T(8,128)(2,1)S(1)} %copy-done.2), kind=kOutput, calls=%fused_computation.49 | convolution fusion | flops 101105640 | bytes 4636768 | tf_op jit(solution)/shard_map/dot_general | solution.py:157
  159.7 1.2 copy.43
  161.0 5.0 %all-to-all-start.1 = ((bf16[32,4,2048]{2,1,0:T(4,128)(2,1)}), bf16[32,4,2048]{2,1,0:T(4,128)(2,1)S(1)}, u32[]{:S(2)}, u32[]{:S(2)}) async-start(bf16[32,4,2048]{2,1,0:T(4,128)(2,1)} %copy.43), calls=%async_computation.1 | async-start | bytes 1048576 | tf_op jit(solution)/shard_map/all_to_all | solution.py:171
  167.6 10.2 %broadcast_multiply_fusion = (f32[24,16,64,64]{3,2,1,0:T(8,128)}, f32[24,16,64,64]{3,2,1,0:T(8,128)}) fusion(f32[24,16,64]{2,1,0:T(8,128)S(1)} %get-tuple-element.4, f32[24,16,64]{2,1,0:T(8,128)S(1)} %reshape.193, f32[24,16,64]{2,1,0:T(8,128)S(1)} %get-tuple-element.2, f32[24,16,64]{2,1,0:T(8,128)} %bitcast.94), kind=kLoop, calls=%fused_computation.6 | loop fusion | flops 3145728 | bytes 12976128 | tf_op jit(solution)/shard_map/mul | solution.py:57
  177.7 10.8 %mul.247 = f32[24,16,4096]{2,1,0:T(8,128)} reshape(f32[24,16,64,64]{3,2,1,0:T(8,128)} %get-tuple-element.14) | data formatting | bytes 12582912 | tf_op jit(solution)/shard_map/mul | solution.py:57
  188.5 10.9 %mul.246 = f32[24,16,4096]{2,1,0:T(8,128)} reshape(f32[24,16,64,64]{3,2,1,0:T(8,128)} %get-tuple-element.15) | data formatting | bytes 12582912 | tf_op jit(solution)/shard_map/mul | solution.py:56
  199.4 5.3 %mul.206 = f32[24,16,64,64]{3,2,1,0:T(8,128)} broadcast(f32[24,16,64]{2,1,0:T(8,128)S(1)} %copy-done.5), dimensions={0,1,3} | broadcast | bytes 6389760 | tf_op jit(solution)/shard_map/mul | solution.py:55
  204.8 10.9 %mul.244 = f32[24,16,4096]{2,1,0:T(8,128)} reshape(f32[24,16,64,64]{3,2,1,0:T(8,128)} %mul.206) | data formatting | bytes 12582912 | tf_op jit(solution)/shard_map/mul | solution.py:55
  215.6 2.0 fusion.72
  217.8 2.7 fusion.15
  220.5 2.4 convolution_convert_fusion
  223.0 1.0 reshape.189
  224.0 12.2 %all-to-all-start.2 = ((bf16[32,4,2048]{2,1,0:T(4,128)(2,1)}), bf16[32,4,2048]{2,1,0:T(4,128)(2,1)S(1)}, u32[]{:S(2)}, u32[]{:S(2)}) async-start(bf16[32,4,2048]{2,1,0:T(4,128)(2,1)} %reshape.189), calls=%async_computation.2 | async-start | bytes 1048576 | tf_op jit(solution)/shard_map/all_to_all | solution.py:176
  236.2 3.0 %fusion.9 = f32[24,2048]{1,0:T(8,128)S(1)} fusion(f32[24,2048]{1,0:T(8,128)S(1)} %get-tuple-element.13, bf16[512,2048]{1,0:T(8,128)(2,1)} %param.45, bf16[2048,512]{1,0:T(8,128)(2,1)} %param.44, f32[24,512]{1,0:T(8,128)S(1)} %fusion.72, f32[2048]{0:T(1024)S(1)} %convert_element_type.160, f32[24]{0:T(128)S(1)} %copy-done.15), kind=kOutput, calls=%fused_computation.16 | convolution fusion | flops 101031936 | bytes 4644960 | tf_op jit(solution)/shard_map/dot_general | solution.py:20
  239.2 14.3 %subtract_add_fusion = f32[24,16,4096]{2,1,0:T(8,128)} fusion(f32[24,16,4096]{2,1,0:T(8,128)} %mul.247, f32[24,16,4096]{2,1,0:T(8,128)} %mul.246, f32[24,16,4096]{2,1,0:T(8,128)} %param.35, f32[24,16,4096]{2,1,0:T(8,128)} %mul.244), kind=kLoop, calls=%fused_computation.5 | loop fusion | flops 4718592 | bytes 31457280 | tf_op jit(solution)/shard_map/add | solution.py:55
  253.5 15.8 %all-to-all-done.2 = bf16[32,4,2048]{2,1,0:T(4,128)(2,1)S(1)} async-done(((bf16[32,4,2048]{2,1,0:T(4,128)(2,1)}), bf16[32,4,2048]{2,1,0:T(4,128)(2,1)S(1)}, u32[]{:S(2)}, u32[]{:S(2)}) %all-to-all-start.2) | async-done | bytes 524320 | tf_op jit(solution)/shard_map/all_to_all | solution.py:176
  269.3 1.1 fusion.7
  (85 shorter events, 16.0 us)
Async XLA Ops:
  7.2 213.4 %copy-start = (bf16[1,512,2048]{2,1,0:T(8,128)(2,1)S(1)}, bf16[1,512,2048]{2,1,0:T(8,128)(2,1)}, u32[]{:S(2)}) copy-start(bf16[1,512,2048]{2,1,0:T(8,128)(2,1)} %param.42) | copy-start | bytes 6291460
  7.2 78.6 %all-gather.2.cloned.1.call-start = ((), (), s32[]{:S(2)}) async-start(), calls=%async_computation.3 | async-start | bytes 3244032 | tf_op jit(solution)/shard_map/all_gather | solution.py:139
  94.2 32.6 %all-to-all-start = ((bf16[32,2,2304]{2,1,0:T(2,128)(2,1)}), bf16[32,2,2304]{2,1,0:T(2,128)(2,1)S(1)}, u32[]{:S(2)}, u32[]{:S(2)}) async-start(bf16[32,2,2304]{2,1,0:T(2,128)(2,1)} %reshape.206), calls=%async_computation | async-start | bytes 589824 | tf_op jit(solution)/shard_map/all_to_all | solution.py:143
  103.6 10.9 %copy-start.16 = (f32[1024]{0:T(1024)S(1)}, f32[1024]{0:T(1024)}, u32[]{:S(2)}) copy-start(f32[1024]{0:T(1024)} %param.31) | copy-start | bytes 12292
  103.6 11.0 %copy-start.17 = (f32[1024]{0:T(1024)S(1)}, f32[1024]{0:T(1024)}, u32[]{:S(2)}) copy-start(f32[1024]{0:T(1024)} %param.32) | copy-start | bytes 12292
  103.6 11.7 %copy-start.18 = (f32[1024]{0:T(1024)S(1)}, f32[1024]{0:T(1024)}, u32[]{:S(2)}) copy-start(f32[1024]{0:T(1024)} %param.33) | copy-start | bytes 12292
  103.7 11.7 %copy-start.19 = (f32[1024]{0:T(1024)S(1)}, f32[1024]{0:T(1024)}, u32[]{:S(2)}) copy-start(f32[1024]{0:T(1024)} %param.34) | copy-start | bytes 12292
  103.7 12.4 %copy-start.20 = (bf16[2048]{0:T(1024)(128)(2,1)S(1)}, bf16[2048]{0:T(1024)(128)(2,1)}, u32[]{:S(2)}) copy-start(bf16[2048]{0:T(1024)(128)(2,1)} %param.37) | copy-start | bytes 12292
  116.8 19.4 %copy-start.13 = (s32[24,4]{0,1:T(4,128)}, s32[24,4]{0,1:T(4,128)S(1)}, u32[]{:S(2)}) copy-start(s32[24,4]{0,1:T(4,128)S(1)} %constant_dynamic-slice_fusion.1) | copy-start | bytes 1156
  117.6 41.8 %copy-start.8 = (s32[24,32]{1,0:T(8,128)}, s32[24,32]{1,0:T(8,128)S(1)}, u32[]{:S(2)}) copy-start(s32[24,32]{1,0:T(8,128)S(1)} %convert_subtract_fusion) | copy-start | bytes 9220
  136.4 8.9 %copy-start.4 = (f32[24,16,64]{2,1,0:T(8,128)}, f32[24,16,64]{2,1,0:T(8,128)S(1)}, u32[]{:S(2)}) copy-start(f32[24,16,64]{2,1,0:T(8,128)S(1)} %fusion.41) | copy-start | bytes 294916
  137.2 8.2 %copy-start.1 = (f32[24,16,64,64]{3,2,1,0:T(8,128)S(1)}, f32[24,16,64,64]{3,2,1,0:T(8,128)}, u32[]{:S(2)}) copy-start(f32[24,16,64,64]{3,2,1,0:T(8,128)} %reshape.185) | copy-start | bytes 18874372
  137.2 8.1 %copy-start.7 = (bf16[24,16,64,1]{2,3,1,0:T(2,128)(2,1)S(1)}, bf16[24,16,64,1]{2,3,1,0:T(2,128)(2,1)}, u32[]{:S(2)}) copy-start(bf16[24,16,64,1]{2,3,1,0:T(2,128)(2,1)} %reshape.205) | copy-start | bytes 147460
  145.3 9.7 %copy-start.3 = (f32[24,16,1,64]{3,2,1,0:T(1,128)}, f32[24,16,1,64]{3,2,1,0:T(1,128)S(1)}, u32[]{:S(2)}) copy-start(f32[24,16,1,64]{3,2,1,0:T(1,128)S(1)} %fusion.74) | copy-start | bytes 294916
  145.4 10.0 %copy-start.6 = (bf16[24,16,64]{2,1,0:T(8,128)(2,1)S(1)}, bf16[24,16,64]{2,1,0:T(8,128)(2,1)}, u32[]{:S(2)}) copy-start(bf16[24,16,64]{2,1,0:T(8,128)(2,1)} %reshape.186) | copy-start | bytes 147460
  145.4 10.0 %copy-start.10 = (f32[16,64]{1,0:T(8,128)S(1)}, f32[16,64]{1,0:T(8,128)}, u32[]{:S(2)}) copy-start(f32[16,64]{1,0:T(8,128)} %mul.222) | copy-start | bytes 12292
  145.4 10.9 %copy-start.2 = (bf16[24,2048]{1,0:T(8,128)(2,1)S(1)}, bf16[24,2048]{1,0:T(8,128)(2,1)}, u32[]{:S(2)}) copy-start(bf16[24,2048]{1,0:T(8,128)(2,1)} %param.23) | copy-start | bytes 294916
  155.0 4.3 %copy-start.11 = (pred[24,32]{1,0:T(8,128)(4,1)S(1)}, pred[24,32]{1,0:T(8,128)(4,1)}, u32[]{:S(2)}) copy-start(pred[24,32]{1,0:T(8,128)(4,1)} %get-tuple-element.10) | copy-start | bytes 2308
  159.3 56.3 %copy-start.14 = (f32[24]{0:T(128)}, f32[24]{0:T(128)S(1)}, u32[]{:S(2)}) copy-start(f32[24]{0:T(128)S(1)} %add_rsqrt_fusion.2) | copy-start | bytes 292
  161.0 56.7 %all-to-all-start.1 = ((bf16[32,4,2048]{2,1,0:T(4,128)(2,1)}), bf16[32,4,2048]{2,1,0:T(4,128)(2,1)S(1)}, u32[]{:S(2)}, u32[]{:S(2)}) async-start(bf16[32,4,2048]{2,1,0:T(4,128)(2,1)} %copy.43), calls=%async_computation.1 | async-start | bytes 1048576 | tf_op jit(solution)/shard_map/all_to_all | solution.py:171
  188.5 10.9 %copy-start.5 = (f32[24,16,64]{2,1,0:T(8,128)S(1)}, f32[24,16,64]{2,1,0:T(8,128)}, u32[]{:S(2)}) copy-start(f32[24,16,64]{2,1,0:T(8,128)} %copy-done.4) | copy-start | bytes 294916
  217.6 18.5 %copy-start.15 = (f32[24]{0:T(128)S(1)}, f32[24]{0:T(128)}, u32[]{:S(2)}) copy-start(f32[24]{0:T(128)} %copy-done.14) | copy-start | bytes 292
  224.0 45.3 %all-to-all-start.2 = ((bf16[32,4,2048]{2,1,0:T(4,128)(2,1)}), bf16[32,4,2048]{2,1,0:T(4,128)(2,1)S(1)}, u32[]{:S(2)}, u32[]{:S(2)}) async-start(bf16[32,4,2048]{2,1,0:T(4,128)(2,1)} %reshape.189), calls=%async_computation.2 | async-start | bytes 1048576 | tf_op jit(solution)/shard_map/all_to_all | solution.py:176
  239.2 30.1 %copy-start.9 = (s32[24,32]{1,0:T(8,128)S(1)}, s32[24,32]{1,0:T(8,128)}, u32[]{:S(2)}) copy-start(s32[24,32]{1,0:T(8,128)} %copy-done.8) | copy-start | bytes 9220
  239.2 30.1 %copy-start.12 = (pred[24,32]{1,0:T(8,128)(4,1)S(1)}, pred[24,32]{1,0:T(8,128)(4,1)}, u32[]{:S(2)}) copy-start(pred[24,32]{1,0:T(8,128)(4,1)} %get-tuple-element.10) | copy-start | bytes 2308
Sparse Core Ops, SparseCore 0:
  10.9 74.8 all-gather.1
where the time goes:
time: 280 us; the launch traced here: 277 us
  waiting for transfers between devices  94.6 us (34%)
  local copies, waits for them, and re-layouts  73.5 us (26%)
  matrix products  35.4 us (13%)
  other arithmetic  32.7 us (12%)
  starting transfers between devices  26.6 us (10%)
  between operations  14.4 us (5%)
    all_gather x1, waiting for transfers between devices, per_device(): lax.all_gather(normed, 'ep', axis=0, tiled=True)  69.5 us
    mul x2, local copies, waits for them, and re-layouts, attention_mixer(): matrix * heads(decay)[:, :, None, :]  16.2 us
    all_to_all x1, waiting for transfers between devices, per_device(): lax.all_to_all(output, 'ep', split_axis=0, concat_axis=0, tiled=True)  15.8 us
    add x1, other arithmetic, attention_mixer(): matrix * heads(decay)[:, :, None, :]  14.3 us
    all_to_all x1, starting transfers between devices, per_device(): lax.all_to_all(output, 'ep', split_axis=0, concat_axis=0, tiled=True)  12.2 us
    reshape x1, local copies, waits for them, and re-layouts, attention_mixer(): matrix = head_state.reshape(tally_value, HEAD_COUNT, HEAD_SIZE, HEAD_SIZE)  10.9 us
    mul x1, local copies, waits for them, and re-layouts, attention_mixer(): recalled[..., None] * removal[:, :, None, :]  10.9 us
    mul x1, local copies, waits for them, and re-layouts, attention_mixer(): head_value[..., None] * rate_scaled_key[:, :, None, :]  10.8 us
  transfers between devices with their start and end apart: 4, of which 3 were waited for; matrix products, arithmetic and copies ran while one was open for 32% of the time, Pallas kernels for 0%

commit v1 on v0

v1 whole, which is shorter than its diff:
```python
import functools

import jax
import jax.numpy as jnp
from jax import lax
from jax.experimental import pallas as pl
from jax.experimental.pallas import tpu as pltpu
from jax.sharding import PartitionSpec as P

HEAD_COUNT = 16
HEAD_SIZE = 64
ROLES = 6
PIECES = 2
PAD = 32
TOKEN_BLOCK = 8
MESH = pl.DeviceIdType.MESH
F32 = jnp.float32
BF16 = jnp.bfloat16


def iota(shape, dim):
    return lax.broadcasted_iota(jnp.int32, shape, dim)


def norm_rows(rows, gain):
    scale = lax.rsqrt(jnp.mean(rows * rows, axis=-1, keepdims=True) + 1e-06)
    return (rows * scale * gain).astype(BF16)


def mm(a, b):
    return jnp.dot(a, b, preferred_element_type=F32)


def ring_of(size):
    ep = lax.axis_index("ep")
    chips = size // 2
    z, core = ep // 2, lax.rem(ep, 2)

    def at(offset):
        return {"ep": lax.rem(z + offset + chips, chips) * 2 + core}

    return z, core, at, {"ep": z * 2 + 1 - core}


def rcopy(src, dst, send, recv, dev):
    return pltpu.make_async_remote_copy(
        src_ref=src, dst_ref=dst, send_sem=send, recv_sem=recv, device_id=dev, device_id_type=MESH
    )


class Gather:
    def __init__(self, slots, rows, send, recv, at, half):
        self.slots, self.rows, self.send, self.recv, self.at, self.half = slots, rows, send, recv, at, half

    def view(self, s, d, p):
        return self.slots.at[s - 1, d, p, pl.ds(0, self.rows)]

    def copy(self, s, d, p):
        last = isinstance(s, int) and s == self.half
        own = isinstance(s, int) and s == 1
        src = self.view(self.half, 1, p) if own else self.view(s - 1, d, p)
        dst = self.view(s, 0 if last else d, p)
        return rcopy(src, dst, self.send.at[s - 1, d, p], self.recv.at[s - 1, d, p], self.at(1 if d == 0 else -1))

    def has(self, s, d, p):
        return not (isinstance(s, int) and s == self.half) or (p < PIECES // 2) == (d == 0)

    def start(self, s, p):
        for d in range(2):
            if self.has(s, d, p):
                self.copy(s, d, p).start()

    def wait(self, s, p):
        for d in range(2):
            if self.has(s, d, p):
                self.copy(s, d, p).wait_recv()

    def drain(self):
        for s in range(1, self.half + 1):
            for d in range(2):
                for p in range(PIECES):
                    if self.has(s, d, p):
                        self.copy(s, d, p).wait_send()


def project_kernel(
    size,
    x_ref,
    gain_ref,
    w0,
    w1,
    w2,
    w3,
    w4,
    w5,
    eg_ref,
    eu_ref,
    ed_ref,
    out_ref,
    sg_ref,
    su_ref,
    sd_ref,
    raw,
    wx,
    perm,
    slots,
    stage,
    land,
    load_sem,
    swap_send,
    swap_recv,
    g_send,
    g_recv,
    a_send,
    a_recv,
):
    z, core, at, sibling = ring_of(size)
    rows, width = x_ref.shape
    half = size // 4
    part = width // PIECES
    cols = w0.shape[1]
    loads = [pltpu.make_async_copy(w, raw.at[i], load_sem.at[i]) for i, w in enumerate((w0, w1, w2, w3, w4, w5))]
    for load in loads:
        load.start()
    barrier = pltpu.get_barrier_semaphore()
    for dev in (at(-1), at(1), sibling):
        pl.semaphore_signal(barrier, inc=1, device_id=dev, device_id_type=MESH)
    normed = norm_rows(x_ref[...].astype(F32), gain_ref[...].astype(F32))
    for p in range(PIECES):
        slots[half - 1, 1, p, 0:rows] = normed[:, p * part : (p + 1) * part]
    pl.semaphore_wait(barrier, 3)
    gather = Gather(slots, rows, g_send, g_recv, at, half)
    for p in range(PIECES):
        gather.start(1, p)
    swaps = [
        rcopy(src, dst, swap_send.at[i + 1], swap_recv.at[i + 1], sibling)
        for i, (src, dst) in enumerate(((eg_ref, sg_ref), (eu_ref, su_ref), (ed_ref, sd_ref)))
    ]
    for i, load in enumerate(loads):
        load.wait()
        wx[core, :, i * cols : (i + 1) * cols] = raw[i]
    swap = rcopy(wx.at[core], wx.at[core], swap_send.at[0], swap_recv.at[0], sibling)
    swap.start()
    for copy in swaps:
        copy.start()
    count = ROLES * cols
    for k in range(2):
        i, j = iota((count, 2 * count), 0), iota((count, 2 * count), 1)
        role = (i * (65536 // cols + 1)) >> 16
        perm[k] = jnp.where(j == i + role * cols + k * cols, 1.0, 0.0).astype(BF16)
    other = rcopy(wx.at[1 - core], wx.at[1 - core], swap_send.at[0], swap_recv.at[0], sibling)

    def project(s):
        done = None
        for k in range(2):
            acc = None
            for p in range(PIECES):
                term = mm(slots[s - 1, :, p].reshape(2 * PAD, part), wx[k, p * part : (p + 1) * part, :])
                acc = term if acc is None else acc + term
            moved = mm(acc.astype(BF16), perm[k])
            done = moved if done is None else done + moved
        stage[s - 1] = done.astype(BF16).reshape(2, PAD, 2 * count)

    def deliver(s, d):
        return rcopy(
            stage.at[s - 1, d, pl.ds(0, rows)], land.at[z], a_send.at[s - 1, d], a_recv.at[s - 1, d], at(-s if d == 0 else s)
        )

    for p in range(PIECES):
        gather.wait(1, p)
        gather.start(2, p)
    other.wait_recv()
    project(1)
    deliver(1, 0).start()
    deliver(1, 1).start()

    def step(s, carry):
        for p in range(PIECES):
            gather.wait(s, p)
            gather.start(s + 1, p)
        project(s)
        deliver(s, 0).start()
        deliver(s, 1).start()
        return carry

    lax.fori_loop(2, half - 1, step, 0)
    for p in range(PIECES):
        gather.wait(half - 1, p)
        gather.start(half, p)
    project(half - 1)
    deliver(half - 1, 0).start()
    deliver(half - 1, 1).start()
    for p in range(PIECES):
        gather.wait(half, p)
    project(half)
    deliver(half, 0).start()
    land[z] = stage[half - 1, 1, 0:rows]
    gather.drain()
    swap.wait_send()
    for copy in swaps:
        copy.wait()
    for s in range(1, half + 1):
        for d in range(2):
            if s < half or d == 0:
                deliver(s, d).wait()
    out_ref[...] = land[...]


def sigmoid(v):
    return 1.0 / (1.0 + jnp.exp(-v))


def state_kernel(
    r_ref, prm_ref, x_ref, wo_ref, s_ref, ns_ref, mid_ref, rt, tt, vecs, vals, gate, self_s, blk, exp_m, red_m, mixed, xcat, wo, wo_sem
):
    step, steps = pl.program_id(0), pl.num_programs(0)
    tokens = x_ref.shape[0]
    total = tokens * HEAD_COUNT
    two = 2 * HEAD_SIZE
    load = pltpu.make_async_copy(wo_ref, wo, wo_sem)

    @pl.when(step == 0)
    def _():
        load.start()
        for i in range(3):
            rt[i] = r_ref[:, :, i * two : (i + 1) * two].astype(F32).reshape(total, two)
        for i in range(3):
            for t in range(tokens):
                tt[i, t * HEAD_COUNT : (t + 1) * HEAD_COUNT] = rt[i, pl.ds(t, HEAD_COUNT, stride=tokens), :]
        low = iota((total, two), 1) < HEAD_SIZE

        def split(i):
            a = tt[i]
            b = pltpu.roll(a, HEAD_SIZE, 1)
            return jnp.where(low, a, b), jnp.where(low, b, a)

        def param(i):
            v = prm_ref[i]
            v = jnp.concatenate([v, v], axis=1)
            return jnp.broadcast_to(v[None], (tokens, HEAD_COUNT, two)).reshape(total, two)

        rr, kk = split(0)
        vv, dd = split(1)
        ta, gg = split(2)
        decay = jnp.exp(-0.6065306597126334 * sigmoid(param(0) + dd))
        rate = sigmoid(param(1) + ta)
        rs = lax.rsqrt(1.0 + 0.5 * jnp.sum(kk * kk, axis=-1, keepdims=True))
        sk = kk * rate
        vecs[0] = -(rs * rs) * kk
        vecs[1] = decay
        vecs[2] = sk
        vecs[3] = rr
        vals[...] = vv.astype(BF16)
        self_s[...] = 0.5 * jnp.sum(rr * sk * param(2), axis=-1, keepdims=True) * vv
        gate[...] = sigmoid(gg)
        i, j = iota((256, 256), 0), iota((256, 256), 1)
        blk[...] = jnp.where((i >> 6) == (j >> 6), 1.0, 0.0).astype(BF16)
        i, j = iota((two, HEAD_SIZE * HEAD_SIZE), 0), iota((two, HEAD_SIZE * HEAD_SIZE), 1)
        exp_m[...] = jnp.where((j >> 6) == i, 1.0, 0.0).astype(BF16)
        i, j = iota((HEAD_SIZE * HEAD_SIZE, two), 0), iota((HEAD_SIZE * HEAD_SIZE, two), 1)
        red_m[...] = jnp.where((i >> 6) == (j & (HEAD_SIZE - 1)), 1.0, 0.0).astype(BF16)

    block = s_ref.shape[0]
    m = block * HEAD_COUNT
    at = pl.ds(pl.multiple_of(step * m, m), m)

    def wide(i):
        v = vecs[i, at, :]
        return jnp.concatenate([v, v], axis=1)

    u2, dec, sk, rr = wide(0), wide(1), wide(2), wide(3)
    val = vals[at, :]
    read = jnp.zeros((m, two), F32)
    for jj in range(HEAD_SIZE * HEAD_SIZE // 256):
        ls = slice(jj * 256, (jj + 1) * 256)
        s = s_ref[:, :, ls].reshape(m, 256)
        comb = mm((s * u2).astype(BF16), blk[...]) + mm(val, exp_m[:, ls])
        new = s * dec + sk * comb
        ns_ref[:, :, ls] = new.reshape(block, HEAD_COUNT, 256)
        read = read + mm((new * rr).astype(BF16), red_m[ls, :])
    centered = read - jnp.mean(read, axis=-1, keepdims=True)
    var = jnp.mean(centered * centered, axis=-1, keepdims=True)
    gain = jnp.concatenate([prm_ref[3], prm_ref[3]], axis=1)
    gain = jnp.broadcast_to(gain[None], (block, HEAD_COUNT, two)).reshape(m, two)
    mixed[at, :] = (centered * lax.rsqrt(var + 0.00064) * gain + self_s[at, :]) * gate[at, :]

    @pl.when(step == steps - 1)
    def _():
        low = iota((tokens, two), 1) < HEAD_SIZE
        for h in range(0, HEAD_COUNT, 2):
            a = mixed[pl.ds(h, tokens, stride=HEAD_COUNT), :]
            b = mixed[pl.ds(h + 1, tokens, stride=HEAD_COUNT), :]
            xcat[:, h * HEAD_SIZE : h * HEAD_SIZE + two] = jnp.where(low, a, b)
        load.wait()
        attended = mm(xcat[...].astype(BF16), wo[...]).astype(BF16)
        mid_ref[...] = x_ref[...].astype(F32) + attended.astype(F32)


def silu(v):
    return v * sigmoid(v)


def expert_kernel(
    size,
    mid_ref,
    gain_ref,
    routes_ref,
    rweight_ref,
    eg_ref,
    eu_ref,
    ed_ref,
    sg_ref,
    su_ref,
    sd_ref,
    cg_ref,
    cu_ref,
    cd_ref,
    out_ref,
    wg,
    wu,
    wd,
    slots,
    contrib,
    arrive,
    hidden,
    first,
    coef,
    base,
    load_sem,
    g_send,
    g_recv,
    r_send,
    r_recv,
):
    z, core, at, sibling = ring_of(size)
    rows, width = mid_ref.shape
    half = size // 4
    part = width // PIECES
    loads = []
    for i, group in enumerate(((cg_ref, cu_ref, cd_ref), (eg_ref.at[0], eu_ref.at[0], ed_ref.at[0]), (sg_ref.at[0], su_ref.at[0], sd_ref.at[0]))):
        for j, (src, dst) in enumerate(zip(group, (wg, wu, wd))):
            loads.append(pltpu.make_async_copy(src, dst.at[i], load_sem.at[i, j]))
    for load in loads:
        load.start()
    barrier = pltpu.get_barrier_semaphore()
    for dev in (at(-1), at(1)):
        pl.semaphore_signal(barrier, inc=1, device_id=dev, device_id_type=MESH)
    normed = norm_rows(mid_ref[...], gain_ref[...].astype(F32))
    for p in range(PIECES):
        slots[half - 1, 1, p, 0:rows] = normed[:, p * part : (p + 1) * part]
    pl.semaphore_wait(barrier, 2)
    gather = Gather(slots, rows, g_send, g_recv, at, half)
    for p in range(PIECES):
        gather.start(1, p)

    ep = lax.axis_index("ep")
    for e, expert in enumerate((ep, sibling["ep"])):
        for s in range(1, half + 1):
            for d in range(2):
                chip = at(0 if (s == half and d == 1) else (-s if d == 0 else s))["ep"]
                where = pl.ds(pl.multiple_of(chip * rows, 8), rows)
                hit = routes_ref[where, :] == expert
                w = jnp.sum(jnp.where(hit, rweight_ref[where, :], 0.0), axis=-1, keepdims=True)
                coef[e, ((s - 1) * 2 + d) * PAD : ((s - 1) * 2 + d) * PAD + rows] = w

    def up(e, rows_of, count):
        gate = up_ = None
        for p in range(PIECES):
            r = rows_of(p)
            ks = slice(p * part, (p + 1) * part)
            g, u = mm(r, wg[e, ks, :]), mm(r, wu[e, ks, :])
            gate, up_ = (g, u) if gate is None else (gate + g, up_ + u)
        hidden[0:count] = (silu(gate) * up_).astype(BF16)

    def shared_up():
        for load in loads[0:2]:
            load.wait()
        up(0, lambda p: slots[half - 1, 1, p], PAD)

    def shared_down():
        loads[2].wait()
        out = mm(hidden[0:PAD], wd[0])[0:rows]
        base[...] = mid_ref[...] + out.astype(BF16).astype(F32)

    def expert_up(e, b):
        up(e + 1, lambda p: slots[pl.ds(2 * b, 2), :, p].reshape(4 * PAD, part), 4 * PAD)

    def expert_down(e, b):
        cf = coef[e, pl.ds(pl.multiple_of(b * (4 * PAD), 4 * PAD), 4 * PAD), :]
        for p in range(PIECES):
            for c in range(0, part, 512):
                o = mm(hidden[...], wd[e + 1, :, p * part + c : p * part + c + 512])
                o = o.astype(BF16).astype(F32) * cf
                if e == 0:
                    first[:, p * part + c : p * part + c + 512] = o
                else:
                    o = o + first[:, p * part + c : p * part + c + 512]
                    contrib[pl.ds(2 * b, 2), :, p, :, c : c + 512] = o.astype(BF16).reshape(2, 2, PAD, 512)

    def forward(s, p):
        gather.wait(s, p)
        if not (isinstance(s, int) and s == half):
            gather.start(s + 1, p)

    def turn(s, work):
        for i in range(2):
            for p in range(i * PIECES // 2, (i + 1) * PIECES // 2):
                forward(s, p)
            work[i]()

    turn(1, (shared_up, shared_down))
    for p in range(PIECES):
        forward(2, p)
    for load in loads[3:]:
        load.wait()

    def pair(b, carry):
        for e in range(2):
            turn(2 * b + 3 + e, (functools.partial(expert_up, e, b), functools.partial(expert_down, e, b)))
        return carry

    lax.fori_loop(0, half // 2 - 2, pair, 0)
    b = half // 2 - 2
    for e in range(2):
        turn(2 * b + 3 + e, (functools.partial(expert_up, e, b), functools.partial(expert_down, e, b)))
    b = half // 2 - 1
    for e in range(2):
        expert_up(e, b)
        expert_down(e, b)

    def passed(t, d, p, source):
        return rcopy(
            contrib.at[source - 1, 0 if isinstance(source, int) and source == half else d, p, pl.ds(0, rows)],
            arrive.at[t, d, p, pl.ds(0, rows)],
            r_send.at[t, d, p],
            r_recv.at[t, d, p],
            at(-1 if d == 0 else 1),
        )

    def begins(d, p):
        return (p < PIECES // 2) == (d == 0)

    for p in range(PIECES):
        for d in range(2):
            if begins(d, p):
                passed(0, d, p, half).start()
            else:
                passed(1, d, p, half - 1).start()

    def relay(t, d, p):
        passed(t - 1, d, p, half - t).wait_recv()
        mine = contrib[half - t - 1, d, p, 0:rows].astype(F32)
        contrib[half - t - 1, d, p, 0:rows] = (mine + arrive[t - 1, d, p, 0:rows].astype(F32)).astype(BF16)
        passed(t, d, p, half - t).start()

    for p in range(PIECES):
        for d in range(2):
            if begins(d, p):
                relay(1, d, p)

    def hop(t, carry):
        for p in range(PIECES):
            for d in range(2):
                relay(t, d, p)
        return carry

    lax.fori_loop(2, half, hop, 0)
    for p in range(PIECES):
        for d in range(2):
            passed(half - 1, d, p, 1).wait_recv()
        got = arrive[half - 1, 0, p, 0:rows].astype(F32) + arrive[half - 1, 1, p, 0:rows].astype(F32)
        total = base[:, p * part : (p + 1) * part] + contrib[half - 1, 1, p, 0:rows].astype(F32) + got
        out_ref[:, p * part : (p + 1) * part] = total.astype(BF16)
    gather.drain()
    for p in range(PIECES):
        for d in range(2):
            for t in range(half):
                if t > 0 or begins(d, p):
                    passed(t, d, p, half - t).wait_send()


VM = pl.BlockSpec(memory_space=pltpu.VMEM)
ANY = pl.BlockSpec(memory_space=pl.ANY)
DMA = pltpu.SemaphoreType.DMA


def per_device(
    residual_input,
    attention_norm_gain,
    receptance_weight,
    key_weight,
    value_weight,
    decay_weight,
    correction_rate_weight,
    output_gate_weight,
    decay_offset,
    correction_rate_offset,
    self_term_weight,
    head_read_gain,
    previous_state,
    attention_output_weight,
    feedforward_norm_gain,
    routes,
    routing_weight,
    routed_gate_weight,
    routed_up_weight,
    routed_down_weight,
    common_gate_weight,
    common_up_weight,
    common_down_weight,
):
    size = lax.axis_size("ep")
    half = size // 4
    rows, width = residual_input.shape
    part = width // PIECES
    cols = receptance_weight.shape[1]
    lanes = ROLES * cols
    big = pltpu.CompilerParams
    landed, sib_gate, sib_up, sib_down = pl.pallas_call(
        functools.partial(project_kernel, size),
        out_shape=(
            jax.ShapeDtypeStruct((size // 2, rows, 2 * lanes), BF16),
            jax.ShapeDtypeStruct(routed_gate_weight.shape, BF16),
            jax.ShapeDtypeStruct(routed_up_weight.shape, BF16),
            jax.ShapeDtypeStruct(routed_down_weight.shape, BF16),
        ),
        in_specs=[VM, VM] + [ANY] * 9,
        out_specs=(VM, ANY, ANY, ANY),
        scratch_shapes=[
            pltpu.VMEM((ROLES, width, cols), BF16),
            pltpu.VMEM((2, width, lanes), BF16),
            pltpu.VMEM((2, lanes, 2 * lanes), BF16),
            pltpu.VMEM((half, 2, PIECES, PAD, part), BF16),
            pltpu.VMEM((half, 2, PAD, 2 * lanes), BF16),
            pltpu.VMEM((size // 2, rows, 2 * lanes), BF16),
            DMA((ROLES,)),
            DMA((4,)),
            DMA((4,)),
            DMA((half, 2, PIECES)),
            DMA((half, 2, PIECES)),
            DMA((half, 2)),
            DMA((half, 2)),
        ],
        compiler_params=big(collective_id=0, has_side_effects=True, vmem_limit_bytes=40 << 20),
        name="project",
    )(
        residual_input,
        attention_norm_gain.reshape(1, width),
        receptance_weight,
        key_weight,
        value_weight,
        decay_weight,
        correction_rate_weight,
        output_gate_weight,
        routed_gate_weight,
        routed_up_weight,
        routed_down_weight,
    )
    prm = jnp.stack((decay_offset, correction_rate_offset, self_term_weight, head_read_gain)).reshape(
        4, HEAD_COUNT, HEAD_SIZE
    )
    total = rows * HEAD_COUNT
    two = 2 * HEAD_SIZE
    square = HEAD_SIZE * HEAD_SIZE
    block = pl.BlockSpec((TOKEN_BLOCK, HEAD_COUNT, square), lambda i: (i, 0, 0))

    def whole(shape):
        return pl.BlockSpec(shape, lambda i: (0,) * len(shape))

    next_state, middle = pl.pallas_call(
        state_kernel,
        grid=(rows // TOKEN_BLOCK,),
        out_shape=(
            jax.ShapeDtypeStruct(previous_state.shape, F32),
            jax.ShapeDtypeStruct((rows, width), F32),
        ),
        in_specs=[whole(landed.shape), whole(prm.shape), whole(residual_input.shape), ANY, block],
        out_specs=(block, whole((rows, width))),
        scratch_shapes=[
            pltpu.VMEM((3, total, two), F32),
            pltpu.VMEM((3, total, two), F32),
            pltpu.VMEM((4, total, two), F32),
            pltpu.VMEM((total, two), BF16),
            pltpu.VMEM((total, two), F32),
            pltpu.VMEM((total, two), F32),
            pltpu.VMEM((256, 256), BF16),
            pltpu.VMEM((two, square), BF16),
            pltpu.VMEM((square, two), BF16),
            pltpu.VMEM((total, two), F32),
            pltpu.VMEM((rows, HEAD_COUNT * HEAD_SIZE), F32),
            pltpu.VMEM(attention_output_weight.shape, BF16),
            DMA,
        ],
        compiler_params=big(dimension_semantics=("arbitrary",), vmem_limit_bytes=40 << 20),
        name="state",
    )(landed, prm, residual_input, attention_output_weight, previous_state)
    inner = routed_gate_weight.shape[2]
    hidden_out = pl.pallas_call(
        functools.partial(expert_kernel, size),
        out_shape=jax.ShapeDtypeStruct((rows, width), BF16),
        in_specs=[VM] * 4 + [ANY] * 9,
        out_specs=VM,
        scratch_shapes=[
            pltpu.VMEM((3, width, inner), BF16),
            pltpu.VMEM((3, width, inner), BF16),
            pltpu.VMEM((3, inner, width), BF16),
            pltpu.VMEM((half, 2, PIECES, PAD, part), BF16),
            pltpu.VMEM((half, 2, PIECES, PAD, part), BF16),
            pltpu.VMEM((half, 2, PIECES, PAD, part), BF16),
            pltpu.VMEM((4 * PAD, inner), BF16),
            pltpu.VMEM((4 * PAD, width), F32),
            pltpu.VMEM((2, 2 * half * PAD, 1), F32),
            pltpu.VMEM((rows, width), F32),
            DMA((3, 3)),
            DMA((half, 2, PIECES)),
            DMA((half, 2, PIECES)),
            DMA((half, 2, PIECES)),
            DMA((half, 2, PIECES)),
        ],
        compiler_params=big(collective_id=1, has_side_effects=True, vmem_limit_bytes=52 << 20),
        name="experts",
    )(
        middle,
        feedforward_norm_gain.reshape(1, width),
        routes,
        routing_weight,
        routed_gate_weight,
        routed_up_weight,
        routed_down_weight,
        sib_gate,
        sib_up,
        sib_down,
        common_gate_weight,
        common_up_weight,
        common_down_weight,
    )
    return (hidden_out, next_state)


def solution(mesh):
    return jax.shard_map(
        per_device,
        mesh=mesh,
        in_specs=(
            P(("grp", "ep"), None),
            P(),
            P(None, "ep"),
            P(None, "ep"),
            P(None, "ep"),
            P(None, "ep"),
            P(None, "ep"),
            P(None, "ep"),
            P(),
            P(),
            P(),
            P(),
            P(("grp", "ep"), None, None),
            P(),
            P(),
            P("grp", None),
            P("grp", None),
            P("ep", None, None),
            P("ep", None, None),
            P("ep", None, None),
            P(),
            P(),
            P(),
        ),
        out_specs=(P(("grp", "ep"), None), P(("grp", "ep"), None, None)),
        check_vma=False,
    )
```

time: 280 us -> 161 us (0.57)
  Pallas kernels: 0 us -> 135 us
  waiting for transfers between devices: 94.6 us -> 0 us
  local copies, waits for them, and re-layouts: 73.5 us -> 24.4 us
  matrix products: 35.4 us -> 0 us
  other arithmetic: 32.7 us -> 0.01 us
  starting transfers between devices: 26.6 us -> 0 us
  between operations: 14.4 us -> 0.81 us
    pallas_call x0 -> x3, Pallas kernels: none -> 135 us  [the longest x1 66.6 us: per_device(): pl.pallas_call(functools.partial(expert_kernel, size), out_shape=jax.Shap...]
    all_gather x1 -> x0, waiting for transfers between devices: 69.5 us -> none  [per_device(): lax.all_gather(normed, 'ep', axis=0, tiled=True)]
    mul x6 -> x0, local copies, waits for them, and re-layouts: 38.6 us -> none  [the longest x2 16.2 us: attention_mixer(): matrix * heads(decay)[:, :, None, :]]
    dot_general x9 -> x0, matrix products: 32.3 us -> none  [the longest x1 9.63 us: attention_mixer(): read = jnp.einsum('nhvk,nhk->nhv', matrix, receptance_head)]
    all_to_all x3 -> x0, starting transfers between devices: 26.6 us -> none  [the longest x1 12.2 us: per_device(): lax.all_to_all(output, 'ep', split_axis=0, concat_axis=0, tiled=True)]
    all_to_all x3 -> x0, waiting for transfers between devices: 25 us -> none  [the longest x1 15.8 us: per_device(): lax.all_to_all(output, 'ep', split_axis=0, concat_axis=0, tiled=True)]
    add x1 -> x0, other arithmetic: 14.3 us -> none  [attention_mixer(): matrix * heads(decay)[:, :, None, :]]
    reshape x6 -> x2, local copies, waits for them, and re-layouts: 13.7 us -> 0.01 us  [the longest x1 0.01 us: per_device(): feedforward_norm_gain.reshape(1, width)]
  transfers between devices with their start and end apart: 4 -> 0, of which waited for: 3 -> 0; matrix products, arithmetic and copies ran while one was open for 32% -> 0% of each run, Pallas kernels for 0% -> 0%
where the time goes in v1:
time: 161 us; the launch traced here: 160 us
  Pallas kernels  135 us (84%)
  local copies, waits for them, and re-layouts  24.4 us (15%)
    pallas_call x1, Pallas kernels, per_device(): pl.pallas_call(functools.partial(expert_kernel, size), out_shape=jax.Shap...  66.6 us
    pallas_call x1, Pallas kernels, per_device(): pl.pallas_call(functools.partial(project_kernel, size), out_shape=(jax.Sh...  54.8 us
    unnamed x53, local copies, waits for them, and re-layouts  24.1 us
    pallas_call x1, Pallas kernels, per_device(): pl.pallas_call(state_kernel, grid=(rows // TOKEN_BLOCK,), out_shape=(jax....  13.5 us

profile of v1, /device:TPU:86, one launch (start us, length us, event | category | flops | bytes accessed | tf_op | source)
XLA Modules:
  0.0 160.1 jit_solution(2368099645471559165)
XLA Ops:
  0.6 0.0 copy-start.12
  0.6 0.0 copy-start.13
  0.7 0.0 copy-start
  0.7 1.3 copy.25.w0
  2.0 1.2 copy.26.w1
  3.2 1.9 %copy.27.w2 = bf16[2048,32]{1,0:T(8,128)(2,1)} copy(bf16[2048,32]{0,1:T(8,128)(2,1)} %param.27) | data formatting | bytes 262144 | tf_op args[4]
  5.1 1.9 %copy.28.w3 = bf16[2048,32]{1,0:T(8,128)(2,1)} copy(bf16[2048,32]{0,1:T(8,128)(2,1)} %param.28) | data formatting | bytes 262144 | tf_op args[5]
  7.0 1.0 copy.29.w4
  8.0 1.0 copy.30.w5
  9.1 0.0 copy-start.1
  9.1 1.6 copy-done.1
  10.7 1.0 copy-done.7
  11.7 1.0 copy-done.8
  12.8 1.0 copy-done.9
  13.8 1.0 copy-done.10
  14.9 54.8 %project.1 = (bf16[16,24,384]{2,1,0:T(8,128)(2,1)S(1)}, bf16[1,2048,512]{2,1,0:T(8,128)(2,1)S(1)}, bf16[1,2048,512]{2,1,0:T(8,128)(2,1)S(1)}, bf16[1,512,2048]{2,1,0:T(8,128)(2,1)S(1)}) custom-call(bf16[24,2048]{1,0:T(8,128)(2,1)S(1)} %copy-done.11, bf16[1,2048]{1,0:T(2,128)(2,1)S(1)} %reshape.19.gain_ref, bf16[2048,32]{1,0:T(8,128)(2,1)S(1)} %copy.25.w0, ...), custom_call_target="tpu_custom_call" | custom-call | tf_op jit(solution)/shard_map/project/pallas_call | solution.py:519
  69.6 0.0 copy-start.4
  69.7 1.3 copy-done.4
  71.0 1.3 copy-done.5
  72.3 1.3 copy-done.6
  73.6 0.1 stack.15
  73.7 0.0 copy-done.18
  73.7 0.1 stack.16
  73.8 0.1 stack.17
  73.8 0.1 stack.18
  73.9 2.8 %copy-done.2 = f32[24,16,4096]{2,1,0:T(8,128)S(1)} copy-done((f32[24,16,4096]{2,1,0:T(8,128)S(1)}, f32[24,16,4096]{2,1,0:T(8,128)}, u32[]{:S(2)}) %copy-start.2) | copy-done | bytes 6291480
  76.7 2.2 %copy-done.3 = bf16[1024,2048]{1,0:T(8,128)(2,1)S(1)} copy-done((bf16[1024,2048]{1,0:T(8,128)(2,1)S(1)}, bf16[1024,2048]{1,0:T(8,128)(2,1)}, u32[]{:S(2)}) %copy-start.3) | copy-done | bytes 4194328
  78.9 13.5 %state.1 = (f32[24,16,4096]{2,1,0:T(8,128)}, f32[24,2048]{1,0:T(8,128)S(1)}) custom-call(bf16[16,24,384]{2,1,0:T(8,128)(2,1)S(1)} %get-tuple-element.8.r_ref, f32[4,16,64]{2,1,0:T(8,128)S(1)} %pad_maximum_fusion.prm_ref, bf16[24,2048]{1,0:T(8,128)(2,1)S(1)} %copy-done.11, bf16[1024,2048]{1,0:T(8,128)(2,1)S(1)} %copy-done.3, f32[24,16,4096]{2,1,0:T(8,128)S(1)} %copy-done.2), custom_call_target="tpu_custom_call" | custom-call | tf_op jit(solution)/shard_map/state/pallas_call | solution.py:570
  92.5 0.2 copy.31.routes_ref
  92.7 0.2 copy.32.rweight_ref
  92.9 66.6 %experts.1 = bf16[24,2048]{1,0:T(8,128)(2,1)S(1)} custom-call(f32[24,2048]{1,0:T(8,128)S(1)} %get-tuple-element.9.mid_ref, bf16[1,2048]{1,0:T(2,128)(2,1)S(1)} %reshape.20.gain_ref, s32[768,4]{1,0:T(8,128)S(1)} %copy.31.routes_ref, f32[768,4]{1,0:T(8,128)S(1)} %copy.32.rweight_ref, bf16[1,2048,512]{2,1,0:T(8,128)(2,1)} %eg_ref.3, ...), custom_call_target="tpu_custom_call" | custom-call | tf_op jit(solution)/shard_map/experts/pallas_call | solution.py:598
  159.5 0.6 copy.34
  (31 shorter events, 0.1 us)
Async XLA Ops:
  0.6 6.4 %copy-start.12 = (bf16[2048,32]{0,1:T(8,128)(2,1)S(1)}, bf16[2048,32]{0,1:T(8,128)(2,1)}, u32[]{:S(2)}) copy-start(bf16[2048,32]{0,1:T(8,128)(2,1)} %param.29) | copy-start | bytes 393220
  0.6 7.4 %copy-start.13 = (bf16[2048,32]{0,1:T(8,128)(2,1)S(1)}, bf16[2048,32]{0,1:T(8,128)(2,1)}, u32[]{:S(2)}) copy-start(bf16[2048,32]{0,1:T(8,128)(2,1)} %param.30) | copy-start | bytes 393220
  0.7 8.4 %copy-start.16 = (bf16[2048]{0:T(1024)(128)(2,1)S(1)}, bf16[2048]{0:T(1024)(128)(2,1)}, u32[]{:S(2)}) copy-start(bf16[2048]{0:T(1024)(128)(2,1)} %param.24) | copy-start | bytes 12292
  0.7 8.4 %copy-start.11 = (bf16[24,2048]{1,0:T(8,128)(2,1)S(1)}, bf16[24,2048]{1,0:T(8,128)(2,1)}, u32[]{:S(2)}) copy-start(bf16[24,2048]{1,0:T(8,128)(2,1)} %x_ref.3) | copy-start | bytes 294916
  0.7 8.4 %copy-start = (bf16[1,2048,512]{2,1,0:T(8,128)(2,1)S(1)}, bf16[1,2048,512]{2,1,0:T(8,128)(2,1)}, u32[]{:S(2)}) copy-start(bf16[1,2048,512]{2,1,0:T(8,128)(2,1)} %eg_ref.3) | copy-start | bytes 6291460
  9.1 1.6 copy-start.1
  10.7 1.0 copy-start.7
  11.7 1.0 copy-start.8
  12.8 1.0 copy-start.9
  13.8 1.0 copy-start.10
  14.8 58.8 %copy-start.17 = (f32[1024]{0:T(1024)S(1)}, f32[1024]{0:T(1024)}, u32[]{:S(2)}) copy-start(f32[1024]{0:T(1024)} %param.31) | copy-start | bytes 12292
  14.8 58.8 %copy-start.18 = (f32[1024]{0:T(1024)S(1)}, f32[1024]{0:T(1024)}, u32[]{:S(2)}) copy-start(f32[1024]{0:T(1024)} %param.32) | copy-start | bytes 12292
  14.9 58.9 %copy-start.19 = (f32[1024]{0:T(1024)S(1)}, f32[1024]{0:T(1024)}, u32[]{:S(2)}) copy-start(f32[1024]{0:T(1024)} %param.33) | copy-start | bytes 12292
  14.9 59.0 %copy-start.20 = (f32[1024]{0:T(1024)S(1)}, f32[1024]{0:T(1024)}, u32[]{:S(2)}) copy-start(f32[1024]{0:T(1024)} %param.34) | copy-start | bytes 12292
  69.6 1.3 copy-start.4
  71.0 1.3 copy-start.5
  72.3 1.3 copy-start.6
  73.9 2.8 %copy-start.2 = (f32[24,16,4096]{2,1,0:T(8,128)S(1)}, f32[24,16,4096]{2,1,0:T(8,128)}, u32[]{:S(2)}) copy-start(f32[24,16,4096]{2,1,0:T(8,128)} %s_ref.1) | copy-start | bytes 18874372
  76.7 2.2 %copy-start.3 = (bf16[1024,2048]{1,0:T(8,128)(2,1)S(1)}, bf16[1024,2048]{1,0:T(8,128)(2,1)}, u32[]{:S(2)}) copy-start(bf16[1024,2048]{1,0:T(8,128)(2,1)} %wo_ref.1) | copy-start | bytes 12582916
  78.9 13.6 %copy-start.14 = (s32[768,4]{0,1:T(4,128)S(1)}, s32[768,4]{0,1:T(4,128)}, u32[]{:S(2)}) copy-start(s32[768,4]{0,1:T(4,128)} %param.38) | copy-start | bytes 36868
  78.9 13.8 %copy-start.15 = (f32[768,4]{0,1:T(4,128)S(1)}, f32[768,4]{0,1:T(4,128)}, u32[]{:S(2)}) copy-start(f32[768,4]{0,1:T(4,128)} %param.39) | copy-start | bytes 36868
  78.9 14.0 %copy-start.21 = (bf16[2048]{0:T(1024)(128)(2,1)S(1)}, bf16[2048]{0:T(1024)(128)(2,1)}, u32[]{:S(2)}) copy-start(bf16[2048]{0:T(1024)(128)(2,1)} %param.37) | copy-start | bytes 12292

commit v2 on v1

--- a/solution.py
+++ b/solution.py
@@ -10,7 +10,7 @@
 HEAD_COUNT = 16
 HEAD_SIZE = 64
 ROLES = 6
-PIECES = 2
+PIECES = 4
 PAD = 32
 TOKEN_BLOCK = 8
 MESH = pl.DeviceIdType.MESH
@@ -97,12 +97,14 @@
     eu_ref,
     ed_ref,
     out_ref,
+    blk_ref,
+    exp_ref,
+    red_ref,
     sg_ref,
     su_ref,
     sd_ref,
-    raw,
-    wx,
-    perm,
+    wide,
+    tall,
     slots,
     stage,
     land,
@@ -118,8 +120,13 @@
     rows, width = x_ref.shape
     half = size // 4
     part = width // PIECES
-    cols = w0.shape[1]
-    loads = [pltpu.make_async_copy(w, raw.at[i], load_sem.at[i]) for i, w in enumerate((w0, w1, w2, w3, w4, w5))]
+    cols = w0.shape[0]
+    mine, others = [], []
+    for i in range(ROLES):
+        mine.append(wide.at[pl.ds(pl.multiple_of(i * 2 * cols + core * cols, cols), cols)])
+        others.append(wide.at[pl.ds(pl.multiple_of(i * 2 * cols + (1 - core) * cols, cols), cols)])
+    weights = (w0, w1, w2, w3, w4, w5)
+    loads = [pltpu.make_async_copy(w, mine[i], load_sem.at[i]) for i, w in enumerate(weights)]
     for load in loads:
         load.start()
     barrier = pltpu.get_barrier_semaphore()
@@ -132,73 +139,59 @@
     gather = Gather(slots, rows, g_send, g_recv, at, half)
     for p in range(PIECES):
         gather.start(1, p)
-    swaps = [
-        rcopy(src, dst, swap_send.at[i + 1], swap_recv.at[i + 1], sibling)
+    swaps = [rcopy(w, mine[i], swap_send.at[i], swap_recv.at[i], sibling) for i, w in enumerate(weights)]
+    swaps += [
+        rcopy(src, dst, swap_send.at[ROLES + i], swap_recv.at[ROLES + i], sibling)
         for i, (src, dst) in enumerate(((eg_ref, sg_ref), (eu_ref, su_ref), (ed_ref, sd_ref)))
     ]
-    for i, load in enumerate(loads):
-        load.wait()
-        wx[core, :, i * cols : (i + 1) * cols] = raw[i]
-    swap = rcopy(wx.at[core], wx.at[core], swap_send.at[0], swap_recv.at[0], sibling)
-    swap.start()
     for copy in swaps:
         copy.start()
-    count = ROLES * cols
-    for k in range(2):
-        i, j = iota((count, 2 * count), 0), iota((count, 2 * count), 1)
-        role = (i * (65536 // cols + 1)) >> 16
-        perm[k] = jnp.where(j == i + role * cols + k * cols, 1.0, 0.0).astype(BF16)
-    other = rcopy(wx.at[1 - core], wx.at[1 - core], swap_send.at[0], swap_recv.at[0], sibling)
-
-    def project(s):
-        done = None
-        for k in range(2):
-            acc = None
-            for p in range(PIECES):
-                term = mm(slots[s - 1, :, p].reshape(2 * PAD, part), wx[k, p * part : (p + 1) * part, :])
-                acc = term if acc is None else acc + term
-            moved = mm(acc.astype(BF16), perm[k])
-            done = moved if done is None else done + moved
-        stage[s - 1] = done.astype(BF16).reshape(2, PAD, 2 * count)
+    square, two = red_ref.shape
+    side = blk_ref.shape[0]
+    i, j = iota((side, side), 0), iota((side, side), 1)
+    blk_ref[...] = jnp.where((i >> 6) == (j >> 6), 1.0, 0.0).astype(BF16)
+    i, j = iota((two, square), 0), iota((two, square), 1)
+    exp_ref[...] = jnp.where((j >> 6) == i, 1.0, 0.0).astype(BF16)
+    i, j = iota((square, two), 0), iota((square, two), 1)
+    red_ref[...] = jnp.where((i >> 6) == (j & (HEAD_SIZE - 1)), 1.0, 0.0).astype(BF16)
+    for i in range(ROLES):
+        loads[i].wait()
+        rcopy(weights[i], others[i], swap_send.at[i], swap_recv.at[i], sibling).wait_recv()
+    for k in range(0, width, 256):
+        tall[k : k + 256, :] = wide[:, k : k + 256].T
+
+    def advance(s):
+        acc = None
+        for p in range(PIECES):
+            gather.wait(s, p)
+            if not (isinstance(s, int) and s == half):
+                gather.start(s + 1, p)
+            term = mm(slots[s - 1, :, p].reshape(2 * PAD, part), tall[p * part : (p + 1) * part, :])
+            acc = term if acc is None else acc + term
+        stage[s - 1] = acc.astype(BF16).reshape(2, PAD, 2 * ROLES * cols)
 
     def deliver(s, d):
         return rcopy(
             stage.at[s - 1, d, pl.ds(0, rows)], land.at[z], a_send.at[s - 1, d], a_recv.at[s - 1, d], at(-s if d == 0 else s)
         )
 
-    for p in range(PIECES):
-        gather.wait(1, p)
-        gather.start(2, p)
-    other.wait_recv()
-    project(1)
-    deliver(1, 0).start()
-    deliver(1, 1).start()
-
     def step(s, carry):
-        for p in range(PIECES):
-            gather.wait(s, p)
-            gather.start(s + 1, p)
-        project(s)
+        advance(s)
         deliver(s, 0).start()
         deliver(s, 1).start()
         return carry
 
+    step(1, 0)
     lax.fori_loop(2, half - 1, step, 0)
-    for p in range(PIECES):
-        gather.wait(half - 1, p)
-        gather.start(half, p)
-    project(half - 1)
-    deliver(half - 1, 0).start()
-    deliver(half - 1, 1).start()
-    for p in range(PIECES):
-        gather.wait(half, p)
-    project(half)
+    step(half - 1, 0)
+    advance(half)
     deliver(half, 0).start()
     land[z] = stage[half - 1, 1, 0:rows]
     gather.drain()
-    swap.wait_send()
-    for copy in swaps:
-        copy.wait()
+    for i, copy in enumerate(swaps):
+        copy.wait_send()
+        if i >= ROLES:
+            copy.wait_recv()
     for s in range(1, half + 1):
         for d in range(2):
             if s < half or d == 0:
@@ -211,89 +204,112 @@
 
 
 def state_kernel(
-    r_ref, prm_ref, x_ref, wo_ref, s_ref, ns_ref, mid_ref, rt, tt, vecs, vals, gate, self_s, blk, exp_m, red_m, mixed, xcat, wo, wo_sem
+    r_ref,
+    blk,
+    exp_m,
+    red_m,
+    prm_ref,
+    x_ref,
+    wo_ref,
+    s_ref,
+    ns_ref,
+    mid_ref,
+    olds,
+    news,
+    wo,
+    rt,
+    tt,
+    vecs,
+    vals,
+    gate,
+    self_s,
+    mixed,
+    xcat,
+    in_sem,
+    out_sem,
+    wo_sem,
 ):
-    step, steps = pl.program_id(0), pl.num_programs(0)
     tokens = x_ref.shape[0]
     total = tokens * HEAD_COUNT
     two = 2 * HEAD_SIZE
-    load = pltpu.make_async_copy(wo_ref, wo, wo_sem)
-
-    @pl.when(step == 0)
-    def _():
-        load.start()
-        for i in range(3):
-            rt[i] = r_ref[:, :, i * two : (i + 1) * two].astype(F32).reshape(total, two)
-        for i in range(3):
-            for t in range(tokens):
-                tt[i, t * HEAD_COUNT : (t + 1) * HEAD_COUNT] = rt[i, pl.ds(t, HEAD_COUNT, stride=tokens), :]
-        low = iota((total, two), 1) < HEAD_SIZE
-
-        def split(i):
-            a = tt[i]
-            b = pltpu.roll(a, HEAD_SIZE, 1)
-            return jnp.where(low, a, b), jnp.where(low, b, a)
-
-        def param(i):
-            v = prm_ref[i]
-            v = jnp.concatenate([v, v], axis=1)
-            return jnp.broadcast_to(v[None], (tokens, HEAD_COUNT, two)).reshape(total, two)
-
-        rr, kk = split(0)
-        vv, dd = split(1)
-        ta, gg = split(2)
-        decay = jnp.exp(-0.6065306597126334 * sigmoid(param(0) + dd))
-        rate = sigmoid(param(1) + ta)
-        rs = lax.rsqrt(1.0 + 0.5 * jnp.sum(kk * kk, axis=-1, keepdims=True))
-        sk = kk * rate
-        vecs[0] = -(rs * rs) * kk
-        vecs[1] = decay
-        vecs[2] = sk
-        vecs[3] = rr
-        vals[...] = vv.astype(BF16)
-        self_s[...] = 0.5 * jnp.sum(rr * sk * param(2), axis=-1, keepdims=True) * vv
-        gate[...] = sigmoid(gg)
-        i, j = iota((256, 256), 0), iota((256, 256), 1)
-        blk[...] = jnp.where((i >> 6) == (j >> 6), 1.0, 0.0).astype(BF16)
-        i, j = iota((two, HEAD_SIZE * HEAD_SIZE), 0), iota((two, HEAD_SIZE * HEAD_SIZE), 1)
-        exp_m[...] = jnp.where((j >> 6) == i, 1.0, 0.0).astype(BF16)
-        i, j = iota((HEAD_SIZE * HEAD_SIZE, two), 0), iota((HEAD_SIZE * HEAD_SIZE, two), 1)
-        red_m[...] = jnp.where((i >> 6) == (j & (HEAD_SIZE - 1)), 1.0, 0.0).astype(BF16)
-
-    block = s_ref.shape[0]
+    block = TOKEN_BLOCK
     m = block * HEAD_COUNT
-    at = pl.ds(pl.multiple_of(step * m, m), m)
-
-    def wide(i):
-        v = vecs[i, at, :]
-        return jnp.concatenate([v, v], axis=1)
-
-    u2, dec, sk, rr = wide(0), wide(1), wide(2), wide(3)
-    val = vals[at, :]
-    read = jnp.zeros((m, two), F32)
-    for jj in range(HEAD_SIZE * HEAD_SIZE // 256):
-        ls = slice(jj * 256, (jj + 1) * 256)
-        s = s_ref[:, :, ls].reshape(m, 256)
-        comb = mm((s * u2).astype(BF16), blk[...]) + mm(val, exp_m[:, ls])
-        new = s * dec + sk * comb
-        ns_ref[:, :, ls] = new.reshape(block, HEAD_COUNT, 256)
-        read = read + mm((new * rr).astype(BF16), red_m[ls, :])
-    centered = read - jnp.mean(read, axis=-1, keepdims=True)
-    var = jnp.mean(centered * centered, axis=-1, keepdims=True)
-    gain = jnp.concatenate([prm_ref[3], prm_ref[3]], axis=1)
-    gain = jnp.broadcast_to(gain[None], (block, HEAD_COUNT, two)).reshape(m, two)
-    mixed[at, :] = (centered * lax.rsqrt(var + 0.00064) * gain + self_s[at, :]) * gate[at, :]
-
-    @pl.when(step == steps - 1)
-    def _():
-        low = iota((tokens, two), 1) < HEAD_SIZE
-        for h in range(0, HEAD_COUNT, 2):
-            a = mixed[pl.ds(h, tokens, stride=HEAD_COUNT), :]
-            b = mixed[pl.ds(h + 1, tokens, stride=HEAD_COUNT), :]
-            xcat[:, h * HEAD_SIZE : h * HEAD_SIZE + two] = jnp.where(low, a, b)
-        load.wait()
-        attended = mm(xcat[...].astype(BF16), wo[...]).astype(BF16)
-        mid_ref[...] = x_ref[...].astype(F32) + attended.astype(F32)
+
+    def load(i):
+        return pltpu.make_async_copy(s_ref.at[pl.ds(i * block, block)], olds.at[i], in_sem.at[i])
+
+    def store(i):
+        return pltpu.make_async_copy(news.at[i], ns_ref.at[pl.ds(i * block, block)], out_sem.at[i])
+
+    wo_load = pltpu.make_async_copy(wo_ref, wo, wo_sem)
+    for i in range(tokens // block):
+        load(i).start()
+    wo_load.start()
+    for i in range(3):
+        rt[i] = r_ref[:, :, i * two : (i + 1) * two].astype(F32).reshape(total, two)
+    for i in range(3):
+        for t in range(tokens):
+            tt[i, t * HEAD_COUNT : (t + 1) * HEAD_COUNT] = rt[i, pl.ds(t, HEAD_COUNT, stride=tokens), :]
+    low = iota((total, two), 1) < HEAD_SIZE
+
+    def split(i):
+        a = tt[i]
+        b = pltpu.roll(a, HEAD_SIZE, 1)
+        return jnp.where(low, a, b), jnp.where(low, b, a)
+
+    def param(i, count):
+        v = jnp.concatenate([prm_ref[i], prm_ref[i]], axis=1)
+        return jnp.broadcast_to(v[None], (count, HEAD_COUNT, two)).reshape(count * HEAD_COUNT, two)
+
+    rr, kk = split(0)
+    vv, dd = split(1)
+    ta, gg = split(2)
+    rate = sigmoid(param(1, tokens) + ta)
+    rs = lax.rsqrt(1.0 + 0.5 * jnp.sum(kk * kk, axis=-1, keepdims=True))
+    sk = kk * rate
+    vecs[0] = -(rs * rs) * kk
+    vecs[1] = jnp.exp(-0.6065306597126334 * sigmoid(param(0, tokens) + dd))
+    vecs[2] = sk
+    vecs[3] = rr
+    vals[...] = vv.astype(BF16)
+    self_s[...] = 0.5 * jnp.sum(rr * sk * param(2, tokens), axis=-1, keepdims=True) * vv
+    gate[...] = sigmoid(gg)
+
+    def update(i, carry):
+        load(i).wait()
+        at = pl.ds(pl.multiple_of(i * m, m), m)
+
+        def wide(k):
+            v = vecs[k, at, :]
+            return jnp.concatenate([v, v], axis=1)
+
+        u2, dec, sk, rr = wide(0), wide(1), wide(2), wide(3)
+        val = vals[at, :]
+        read = jnp.zeros((m, two), F32)
+        for jj in range(HEAD_SIZE * HEAD_SIZE // 256):
+            ls = slice(jj * 256, (jj + 1) * 256)
+            s = olds[i, :, :, ls].reshape(m, 256)
+            comb = mm((s * u2).astype(BF16), blk[...]) + mm(val, exp_m[:, ls])
+            new = s * dec + sk * comb
+            news[i, :, :, ls] = new.reshape(block, HEAD_COUNT, 256)
+            read = read + mm((new * rr).astype(BF16), red_m[ls, :])
+        store(i).start()
+        centered = read - jnp.mean(read, axis=-1, keepdims=True)
+        var = jnp.mean(centered * centered, axis=-1, keepdims=True)
+        mixed[at, :] = (centered * lax.rsqrt(var + 0.00064) * param(3, block) + self_s[at, :]) * gate[at, :]
+        return carry
+
+    lax.fori_loop(0, tokens // block, update, 0)
+    low = iota((tokens, two), 1) < HEAD_SIZE
+    for h in range(0, HEAD_COUNT, 2):
+        a = mixed[pl.ds(h, tokens, stride=HEAD_COUNT), :]
+        b = mixed[pl.ds(h + 1, tokens, stride=HEAD_COUNT), :]
+        xcat[:, h * HEAD_SIZE : h * HEAD_SIZE + two] = jnp.where(low, a, b)
+    wo_load.wait()
+    attended = mm(xcat[...].astype(BF16), wo[...]).astype(BF16)
+    mid_ref[...] = x_ref[...].astype(F32) + attended.astype(F32)
+    for i in range(tokens // block):
+        store(i).wait()
 
 
 def silu(v):
@@ -363,12 +379,14 @@
                 w = jnp.sum(jnp.where(hit, rweight_ref[where, :], 0.0), axis=-1, keepdims=True)
                 coef[e, ((s - 1) * 2 + d) * PAD : ((s - 1) * 2 + d) * PAD + rows] = w
 
+    gates, ups, downs = wg, wu, wd
+
     def up(e, rows_of, count):
         gate = up_ = None
         for p in range(PIECES):
             r = rows_of(p)
             ks = slice(p * part, (p + 1) * part)
-            g, u = mm(r, wg[e, ks, :]), mm(r, wu[e, ks, :])
+            g, u = mm(r, gates[e, ks, :]), mm(r, ups[e, ks, :])
             gate, up_ = (g, u) if gate is None else (gate + g, up_ + u)
         hidden[0:count] = (silu(gate) * up_).astype(BF16)
 
@@ -379,7 +397,7 @@
 
     def shared_down():
         loads[2].wait()
-        out = mm(hidden[0:PAD], wd[0])[0:rows]
+        out = mm(hidden[0:PAD], downs[0])[0:rows]
         base[...] = mid_ref[...] + out.astype(BF16).astype(F32)
 
     def expert_up(e, b):
@@ -389,7 +407,7 @@
         cf = coef[e, pl.ds(pl.multiple_of(b * (4 * PAD), 4 * PAD), 4 * PAD), :]
         for p in range(PIECES):
             for c in range(0, part, 512):
-                o = mm(hidden[...], wd[e + 1, :, p * part + c : p * part + c + 512])
+                o = mm(hidden[...], downs[e + 1, :, p * part + c : p * part + c + 512])
                 o = o.astype(BF16).astype(F32) * cf
                 if e == 0:
                     first[:, p * part + c : p * part + c + 512] = o
@@ -480,8 +498,16 @@
 
 
 VM = pl.BlockSpec(memory_space=pltpu.VMEM)
-ANY = pl.BlockSpec(memory_space=pl.ANY)
+HBM = pl.BlockSpec(memory_space=pltpu.HBM)
 DMA = pltpu.SemaphoreType.DMA
+
+
+def far(array):
+    return pltpu.with_memory_space_constraint(array, pltpu.HBM)
+
+
+def cost(us):
+    return pl.CostEstimate(flops=int(us * 2e8), bytes_accessed=int(us * 3e6), transcendentals=0)
 
 
 def per_device(
@@ -516,89 +542,89 @@
     cols = receptance_weight.shape[1]
     lanes = ROLES * cols
     big = pltpu.CompilerParams
-    landed, sib_gate, sib_up, sib_down = pl.pallas_call(
+    two = 2 * HEAD_SIZE
+    square = HEAD_SIZE * HEAD_SIZE
+    landed, blk, exp_m, red_m, sib_gate, sib_up, sib_down = pl.pallas_call(
         functools.partial(project_kernel, size),
         out_shape=(
             jax.ShapeDtypeStruct((size // 2, rows, 2 * lanes), BF16),
-            jax.ShapeDtypeStruct(routed_gate_weight.shape, BF16),
-            jax.ShapeDtypeStruct(routed_up_weight.shape, BF16),
-            jax.ShapeDtypeStruct(routed_down_weight.shape, BF16),
+            jax.ShapeDtypeStruct((256, 256), BF16),
+            jax.ShapeDtypeStruct((two, square), BF16),
+            jax.ShapeDtypeStruct((square, two), BF16),
+            pltpu.HBM(routed_gate_weight.shape, BF16),
+            pltpu.HBM(routed_up_weight.shape, BF16),
+            pltpu.HBM(routed_down_weight.shape, BF16),
         ),
-        in_specs=[VM, VM] + [ANY] * 9,
-        out_specs=(VM, ANY, ANY, ANY),
+        in_specs=[VM, VM] + [HBM] * 9,
+        out_specs=(VM,) * 4 + (HBM,) * 3,
         scratch_shapes=[
-            pltpu.VMEM((ROLES, width, cols), BF16),
-            pltpu.VMEM((2, width, lanes), BF16),
-            pltpu.VMEM((2, lanes, 2 * lanes), BF16),
+            pltpu.VMEM((2 * lanes, width), BF16),
+            pltpu.VMEM((width, 2 * lanes), BF16),
             pltpu.VMEM((half, 2, PIECES, PAD, part), BF16),
             pltpu.VMEM((half, 2, PAD, 2 * lanes), BF16),
             pltpu.VMEM((size // 2, rows, 2 * lanes), BF16),
             DMA((ROLES,)),
-            DMA((4,)),
-            DMA((4,)),
+            DMA((ROLES + 3,)),
+            DMA((ROLES + 3,)),
             DMA((half, 2, PIECES)),
             DMA((half, 2, PIECES)),
             DMA((half, 2)),
             DMA((half, 2)),
         ],
-        compiler_params=big(collective_id=0, has_side_effects=True, vmem_limit_bytes=40 << 20),
+        compiler_params=big(collective_id=0, has_side_effects=True, vmem_limit_bytes=16 << 20),
+        cost_estimate=cost(40),
         name="project",
     )(
         residual_input,
         attention_norm_gain.reshape(1, width),
-        receptance_weight,
-        key_weight,
-        value_weight,
-        decay_weight,
-        correction_rate_weight,
-        output_gate_weight,
-        routed_gate_weight,
-        routed_up_weight,
-        routed_down_weight,
+        far(receptance_weight.T),
+        far(key_weight.T),
+        far(value_weight.T),
+        far(decay_weight.T),
+        far(correction_rate_weight.T),
+        far(output_gate_weight.T),
+        far(routed_gate_weight),
+        far(routed_up_weight),
+        far(routed_down_weight),
     )
     prm = jnp.stack((decay_offset, correction_rate_offset, self_term_weight, head_read_gain)).reshape(
         4, HEAD_COUNT, HEAD_SIZE
     )
     total = rows * HEAD_COUNT
-    two = 2 * HEAD_SIZE
-    square = HEAD_SIZE * HEAD_SIZE
-    block = pl.BlockSpec((TOKEN_BLOCK, HEAD_COUNT, square), lambda i: (i, 0, 0))
-
-    def whole(shape):
-        return pl.BlockSpec(shape, lambda i: (0,) * len(shape))
-
+    blocks = (rows // TOKEN_BLOCK, TOKEN_BLOCK, HEAD_COUNT, square)
     next_state, middle = pl.pallas_call(
         state_kernel,
-        grid=(rows // TOKEN_BLOCK,),
         out_shape=(
             jax.ShapeDtypeStruct(previous_state.shape, F32),
             jax.ShapeDtypeStruct((rows, width), F32),
         ),
-        in_specs=[whole(landed.shape), whole(prm.shape), whole(residual_input.shape), ANY, block],
-        out_specs=(block, whole((rows, width))),
+        in_specs=[VM] * 6 + [HBM] * 2,
+        out_specs=(HBM, VM),
         scratch_shapes=[
+            pltpu.VMEM(blocks, F32),
+            pltpu.VMEM(blocks, F32),
+            pltpu.VMEM(attention_output_weight.shape, BF16),
             pltpu.VMEM((3, total, two), F32),
             pltpu.VMEM((3, total, two), F32),
             pltpu.VMEM((4, total, two), F32),
             pltpu.VMEM((total, two), BF16),
             pltpu.VMEM((total, two), F32),
             pltpu.VMEM((total, two), F32),
-            pltpu.VMEM((256, 256), BF16),
-            pltpu.VMEM((two, square), BF16),
-            pltpu.VMEM((square, two), BF16),
             pltpu.VMEM((total, two), F32),
             pltpu.VMEM((rows, HEAD_COUNT * HEAD_SIZE), F32),
-            pltpu.VMEM(attention_output_weight.shape, BF16),
+            DMA(blocks[:1]),
+            DMA(blocks[:1]),
             DMA,
         ],
-        compiler_params=big(dimension_semantics=("arbitrary",), vmem_limit_bytes=40 << 20),
+        compiler_params=big(vmem_limit_bytes=40 << 20),
+        cost_estimate=cost(8),
         name="state",
-    )(landed, prm, residual_input, attention_output_weight, previous_state)
+    )(landed, blk, exp_m, red_m, prm, residual_input, far(attention_output_weight), far(previous_state))
     inner = routed_gate_weight.shape[2]
     hidden_out = pl.pallas_call(
         functools.partial(expert_kernel, size),
         out_shape=jax.ShapeDtypeStruct((rows, width), BF16),
-        in_specs=[VM] * 4 + [ANY] * 9,
+        in_specs=[VM] * 4 + [HBM] * 9,
         out_specs=VM,
         scratch_shapes=[
             pltpu.VMEM((3, width, inner), BF16),
@@ -617,22 +643,23 @@
             DMA((half, 2, PIECES)),
             DMA((half, 2, PIECES)),
         ],
-        compiler_params=big(collective_id=1, has_side_effects=True, vmem_limit_bytes=52 << 20),
+        compiler_params=big(collective_id=1, has_side_effects=True, vmem_limit_bytes=38 << 20),
+        cost_estimate=cost(50),
         name="experts",
     )(
         middle,
         feedforward_norm_gain.reshape(1, width),
         routes,
         routing_weight,
-        routed_gate_weight,
-        routed_up_weight,
-        routed_down_weight,
-        sib_gate,
-        sib_up,
-        sib_down,
-        common_gate_weight,
-        common_up_weight,
-        common_down_weight,
+        far(routed_gate_weight),
+        far(routed_up_weight),
+        far(routed_down_weight),
+        far(sib_gate),
+        far(sib_up),
+        far(sib_down),
+        far(common_gate_weight),
+        far(common_up_weight),
+        far(common_down_weight),
     )
     return (hidden_out, next_state)
 

time: 161 us -> 132 us (0.82)
  local copies, waits for them, and re-layouts: 24.4 us -> 2.92 us
  Pallas kernels: 135 us -> 128 us
    unnamed x53 -> x21, local copies, waits for them, and re-layouts: 24.1 us -> 1.94 us
    pallas_call x1, Pallas kernels: 66.6 us -> 63.5 us  [per_device(): pl.pallas_call(functools.partial(expert_kernel, size), out_shape=jax.Shap...]
    pallas_call x1, Pallas kernels: 54.8 us -> 52.5 us  [per_device(): pl.pallas_call(functools.partial(project_kernel, size), out_shape=(jax.Sh...]
where the time goes in v2:
time: 132 us
  Pallas kernels  128 us (97%)
  local copies, waits for them, and re-layouts  2.92 us (2%)
    pallas_call x1, Pallas kernels, per_device(): pl.pallas_call(functools.partial(expert_kernel, size), out_shape=jax.Shap...  63.5 us
    pallas_call x1, Pallas kernels, per_device(): pl.pallas_call(functools.partial(project_kernel, size), out_shape=(jax.Sh...  52.5 us
    pallas_call x1, Pallas kernels, per_device(): pl.pallas_call(state_kernel, out_shape=(jax.ShapeDtypeStruct(previous_sta...  12.3 us

profile of v2, /device:TPU:86, one launch (start us, length us, event | category | flops | bytes accessed | tf_op | source)
XLA Modules:
  0.0 132.0 jit_solution(3851455953229469715)
XLA Ops:
  0.6 0.7 reshape.19.gain_ref
  1.3 0.0 copy-start
  1.3 0.9 copy-done
  2.2 0.0 copy-start.4
  2.2 0.0 copy-start.5
  2.2 0.0 copy-start.6
  2.2 0.0 copy-start.7
  2.2 0.0 copy-start.1
  2.2 52.5 %project.1 = (bf16[16,24,384]{2,1,0:T(8,128)(2,1)S(1)}, bf16[256,256]{1,0:T(8,128)(2,1)S(1)}, bf16[128,4096]{1,0:T(8,128)(2,1)S(1)}, bf16[4096,128]{1,0:T(8,128)...) custom-call(bf16[24,2048]{1,0:T(8,128)(2,1)S(1)} %copy-done, ...), custom_call_target="tpu_custom_call" | custom-call | flops 8000000000 | bytes 120000000 | tf_op jit(solution)/shard_map/project/pallas_call | solution.py:547
  54.8 0.0 copy-done.4
  54.8 0.1 stack.15
  54.9 0.0 copy-done.5
  54.9 0.1 stack.16
  54.9 0.0 copy-done.6
  54.9 0.1 stack.17
  55.0 0.0 copy-done.7
  55.0 0.1 stack.18
  55.1 0.0 copy-done.1
  55.1 0.0 copy-start.2
  55.1 0.0 copy-start.3
  55.1 0.0 copy-start.8
  55.1 12.3 %state.1 = (f32[24,16,4096]{2,1,0:T(8,128)}, f32[24,2048]{1,0:T(8,128)S(1)}) custom-call(bf16[16,24,384]{2,1,0:T(8,128)(2,1)S(1)} %get-tuple-element.11.r_ref, bf16[256,256]{1,0:T(8,128)(2,1)S(1)} %get-tuple-element.12.blk, bf16[128,4096]{1,0:T(8,128)(2,1)S(1)} %get-tuple-element.13.exp_m, bf16[4096,128]{1,0:T(8,128)(2,1)S(1)} %get-tuple-element.14.red_m, ...), custom_call_target="tpu_custom_call" | custom-call | flops 1600000000 | bytes 24000000 | tf_op jit(solution)/shard_map/state/pallas_call | solution.py:595
  67.4 0.0 copy-done.2
  67.4 0.2 copy.25.routes_ref
  67.6 0.0 copy-done.3
  67.6 0.2 copy.26.rweight_ref
  67.8 0.0 copy-done.8
  67.9 63.5 %experts.1 = bf16[24,2048]{1,0:T(8,128)(2,1)S(1)} custom-call(f32[24,2048]{1,0:T(8,128)S(1)} %get-tuple-element.15.mid_ref, bf16[1,2048]{1,0:T(2,128)(2,1)S(1)} %reshape.20.gain_ref, s32[768,4]{1,0:T(8,128)S(1)} %copy.25.routes_ref, f32[768,4]{1,0:T(8,128)S(1)} %copy.26.rweight_ref, bf16[1,2048,512]{2,1,0:T(8,128)(2,1)} %eg_ref.3, ...), custom_call_target="tpu_custom_call" | custom-call | flops 10000000000 | bytes 150000000 | tf_op jit(solution)/shard_map/experts/pallas_call | solution.py:624
  131.4 0.6 copy.28
  (2 shorter events, 0.0 us)
Async XLA Ops:
  1.3 0.9 copy-start
  2.2 52.6 %copy-start.4 = (f32[1024]{0:T(1024)S(1)}, f32[1024]{0:T(1024)}, u32[]{:S(2)}) copy-start(f32[1024]{0:T(1024)} %param.31) | copy-start | bytes 12292
  2.2 52.6 %copy-start.5 = (f32[1024]{0:T(1024)S(1)}, f32[1024]{0:T(1024)}, u32[]{:S(2)}) copy-start(f32[1024]{0:T(1024)} %param.32) | copy-start | bytes 12292
  2.2 52.7 %copy-start.6 = (f32[1024]{0:T(1024)S(1)}, f32[1024]{0:T(1024)}, u32[]{:S(2)}) copy-start(f32[1024]{0:T(1024)} %param.33) | copy-start | bytes 12292
  2.2 52.8 %copy-start.7 = (f32[1024]{0:T(1024)S(1)}, f32[1024]{0:T(1024)}, u32[]{:S(2)}) copy-start(f32[1024]{0:T(1024)} %param.34) | copy-start | bytes 12292
  2.2 52.9 %copy-start.1 = (bf16[24,2048]{1,0:T(8,128)(2,1)S(1)}, bf16[24,2048]{1,0:T(8,128)(2,1)}, u32[]{:S(2)}) copy-start(bf16[24,2048]{1,0:T(8,128)(2,1)} %x_ref.3) | copy-start | bytes 294916
  55.1 12.3 %copy-start.2 = (s32[768,4]{0,1:T(4,128)S(1)}, s32[768,4]{0,1:T(4,128)}, u32[]{:S(2)}) copy-start(s32[768,4]{0,1:T(4,128)} %param.38) | copy-start | bytes 36868
  55.1 12.5 %copy-start.3 = (f32[768,4]{0,1:T(4,128)S(1)}, f32[768,4]{0,1:T(4,128)}, u32[]{:S(2)}) copy-start(f32[768,4]{0,1:T(4,128)} %param.39) | copy-start | bytes 36868
  55.1 12.7 %copy-start.8 = (bf16[2048]{0:T(1024)(128)(2,1)S(1)}, bf16[2048]{0:T(1024)(128)(2,1)}, u32[]{:S(2)}) copy-start(bf16[2048]{0:T(1024)(128)(2,1)} %param.37) | copy-start | bytes 12292
